TPU v7x, 256 devices: a whole 4x4x8 slice. The times are simulated.
256 devices in a mesh: ep: 16 (over y, x), tp: 16 (over z, core).
Axes of the slice: x: 4, y: 4, z: 8, core: 2. Of those that a mesh axis runs over, the one named last changes fastest.
Arguments:
- pool_input: bfloat16 [32768, 1024], P('ep', 'tp'), may hold values from -6 to 6
- pool_gain: float32 [1024], P('tp'), may hold values from 0.1 to 1.9
- mix_weight: bfloat16 [1024, 2048], P('tp'), may hold values from -0.1875 to 0.1875
- moe_input: bfloat16 [65536, 2048], P(('ep', 'tp')), may hold values from -6 to 6
- moe_gain: float32 [2048], replicated, may hold values from 0.1 to 1.9
- expert_ids: int32 [65536, 2], P(('ep', 'tp')), may hold values from 0 to 15, as said below
- route_weight: float32 [65536, 2], P(('ep', 'tp')), may hold values from 0.2 to 1
- gate_weight: bfloat16 [16, 2048, 1024], P('ep', None, 'tp'), may hold values from -0.125 to 0.125
- up_weight: bfloat16 [16, 2048, 1024], P('ep', None, 'tp'), may hold values from -0.125 to 0.125
- down_weight: bfloat16 [16, 2048, 1024], P('ep', None, 'tp'), may hold values from -0.1875 to 0.1875
Outputs:
- mixed_out: bfloat16 [32768, 2048], P(('ep', 'tp'))
- moe_out: bfloat16 [65536, 2048], P(('ep', 'tp'))
Inputs may be any that keep to these rules, and one draw needn't show every extreme that they name: `expert_ids`: each row names 2 different experts of one group of 4 consecutive experts. In each aligned block of 256 rows (the rows of one device) no expert is named by more than 48 rows, and some expert is named by exactly 48 rows.
All inputs are finite; a program needn't handle non-finite values.
Results may differ from a plain program's by a relative error of at most 0.012.
Values may be sent and summed in bfloat16 or wider, within the bound.
A program may use at most 128 MiB of HBM per device.

v0:
```python
import jax
import jax.numpy as jnp
from jax import lax
from jax.sharding import PartitionSpec as P

GROUP_CH = 256
EXPERTS = 16
TOP = 2
CAP = 48
eps_norm = 1e-06


def from_behind(shard, axis, by):
    peers = lax.axis_size(axis)
    pairs = [(i, i + by) for i in range(peers) if 0 <= i + by < peers]
    return lax.ppermute(shard, axis, pairs)


def gather_turned(arrays, axis, dims):
    turned = [jnp.moveaxis(a, dim, 0) for a, dim in zip(arrays, dims)]
    both = jnp.concatenate([t.reshape(len(t), -1) for t in turned], axis=1)
    result, at, gathered = (lax.all_gather(both, axis, axis=0, tiled=True), 0, [])
    for t, dim in zip(turned, dims):
        section = result[:, at : at + t[0].size].reshape(-1, *t.shape[1:])
        gathered.append(jnp.moveaxis(section, 0, dim))
        at += t[0].size
    return tuple(gathered)


def in_blocks(shard, dim, peers):
    before, after = (shard.shape[:dim], shard.shape[dim + 1 :])
    return jnp.moveaxis(shard.reshape(*before, peers, -1, *after), dim, 0)


def cut_rows(length, count):
    unit = 8 if length >= 8 * count else 1
    return [length // unit * k // count * unit for k in range(1, count)]


def joined_along(tiles, dim):
    tiles = jnp.moveaxis(tiles, 0, dim)
    dims = tiles.shape
    return tiles.reshape(*dims[:dim], dims[dim] * dims[dim + 1], *dims[dim + 2 :])


def exchange_in_pieces(shard, axis, pieces, split_dim, concat_dim):
    tiles = in_blocks(shard, split_dim, lax.axis_size(axis))
    widest = max(range(1, max(2, tiles.ndim - 1)), key=lambda d: tiles.shape[d])
    gathered = []
    for section in jnp.split(tiles, cut_rows(tiles.shape[widest], pieces), axis=widest):
        if section.size:
            gathered.append(lax.all_to_all(section, axis, split_axis=0, concat_axis=0, tiled=True))
    return joined_along(jnp.concatenate(gathered, axis=widest), concat_dim)


def window_sums(extended, row_count):
    level_sum = extended
    stride = 1
    outputs = []
    for doubling in range(4):
        level_sum = level_sum[stride:] + level_sum[:-stride]
        stride = stride * 2
        outputs.append(level_sum[level_sum.shape[0] - row_count :])
    return outputs


def pool_mixer(pool_input, pool_gain):
    row_count, channels = pool_input.shape
    carried = from_behind(pool_input[row_count - 15 :], "ep", 1)
    extended = jnp.concatenate([carried, pool_input], axis=0).astype(jnp.float32)
    window_list = window_sums(extended, row_count)
    channel_ids = lax.axis_index("tp") * channels + lax.iota(jnp.int32, channels)
    group_ids = channel_ids // GROUP_CH
    position = lax.axis_index("ep") * row_count + lax.iota(jnp.int32, row_count)
    summed = jnp.zeros((row_count, channels), jnp.float32)
    widths = jnp.zeros((channels,), jnp.int32)
    for index_group in range(4):
        inside = group_ids == index_group
        summed = jnp.where(inside[None, :], window_list[index_group], summed)
        widths = jnp.where(inside, 2 ** (index_group + 1), widths)
    counted = jnp.minimum(position[:, None] + 1, widths[None, :]).astype(jnp.float32)
    values = extended[15:]
    return ((summed / counted - values) * pool_gain).astype(jnp.bfloat16)


def route_slots(expert_ids):
    flat_ids = expert_ids.reshape(-1)
    marked = (flat_ids[:, None] == lax.iota(jnp.int32, EXPERTS)[None, :]).astype(jnp.int32)
    before_count = jnp.cumsum(marked, axis=0) - marked
    ranked = jnp.sum(before_count * marked, axis=1)
    return (flat_ids * CAP + ranked).reshape(expert_ids.shape)


def body(
    pool_input,
    pool_gain,
    mix_weight,
    moe_input,
    moe_gain,
    expert_ids,
    route_weight,
    gate_weight,
    up_weight,
    down_weight,
):
    pooled = pool_mixer(pool_input, pool_gain)
    mixed_sum = lax.psum_scatter(
        jnp.dot(pooled, mix_weight, preferred_element_type=jnp.float32).astype(jnp.bfloat16),
        "tp",
        scatter_dimension=0,
        tiled=True,
    )
    inputs = moe_input.astype(jnp.float32)
    scale_rows = lax.rsqrt(jnp.mean(inputs * inputs, axis=-1, keepdims=True) + eps_norm)
    normed = (inputs * scale_rows * moe_gain).astype(jnp.bfloat16)
    slots = route_slots(expert_ids)
    slot_index = lax.iota(jnp.int32, EXPERTS * CAP)
    placing = (
        (slot_index[:, None] == slots[None, :, 0]) | (slot_index[:, None] == slots[None, :, 1])
    ).astype(jnp.bfloat16)
    outgoing = jnp.dot(placing, normed, preferred_element_type=jnp.float32).astype(jnp.bfloat16)
    outgoing = outgoing.reshape(EXPERTS, CAP, normed.shape[1])
    arrived = lax.all_to_all(outgoing, "ep", split_axis=0, concat_axis=1, tiled=True)
    gate_piece, up_piece, down_piece = gather_turned(
        (gate_weight, up_weight, down_weight), "tp", (2, 2, 2)
    )
    gate_part = jnp.einsum("erd,edf->erf", arrived, gate_piece, preferred_element_type=jnp.float32)
    upward = jnp.einsum("erd,edf->erf", arrived, up_piece, preferred_element_type=jnp.float32)
    hidden = (jax.nn.silu(gate_part) * upward).astype(jnp.bfloat16)
    expert_sum = jnp.einsum("erf,edf->erd", hidden, down_piece, preferred_element_type=jnp.float32)
    expert_rows = expert_sum.astype(jnp.bfloat16)
    returned = exchange_in_pieces(expert_rows, "ep", 2, 1, 0)
    returned_rows = returned.reshape(EXPERTS * CAP, returned.shape[2])
    combined = jnp.zeros((normed.shape[0], normed.shape[1]), jnp.float32)
    for route_index in range(TOP):
        picking = (slots[:, route_index][:, None] == slot_index[None, :]).astype(jnp.bfloat16)
        chosen_rows = jnp.dot(picking, returned_rows, preferred_element_type=jnp.float32)
        combined = combined + route_weight[:, route_index : route_index + 1] * chosen_rows
    moe_out = combined.astype(jnp.bfloat16)
    return (mixed_sum, moe_out)


def solution(mesh):
    return jax.shard_map(
        body,
        mesh=mesh,
        in_specs=(
            P("ep", "tp"),
            P("tp"),
            P("tp", None),
            P(("ep", "tp"), None),
            P(),
            P(("ep", "tp"), None),
            P(("ep", "tp"), None),
            P("ep", None, "tp"),
            P("ep", None, "tp"),
            P("ep", None, "tp"),
        ),
        out_specs=(P(("ep", "tp"), None), P(("ep", "tp"), None)),
        check_vma=False,
    )
```

profile of v0, /device:TPU:24, one launch (start us, length us, event | category | flops | bytes accessed | tf_op | source)
XLA Modules:
  0.0 169.4 jit_solution(2128738845076339087)
XLA Ops:
  7.2 2.1 %pad_maximum_fusion.1 = bf16[64,6144]{1,0:T(8,128)(2,1)} fusion(bf16[64,2048]{1,0:T(8,128)(2,1)} %bitcast.76, bf16[64,2048]{1,0:T(8,128)(2,1)} %bitcast.77, bf16[64,2048]{1,0:T(8,128)(2,1)} %bitcast.78), kind=kLoop, calls=%fused_computation.22 | loop fusion | flops 2359296 | bytes 1572864 | tf_op jit(solution)/shard_map/concatenate | solution.py:21
  9.4 0.8 slice.66
  10.2 3.4 %collective-permute-start = (bf16[15,64]{0,1:T(8,128)(2,1)S(1)}, bf16[15,64]{0,1:T(8,128)(2,1)S(1)}, u32[]{:S(2)}, u32[]{:S(2)}) collective-permute-start(bf16[15,64]{0,1:T(8,128)(2,1)S(1)} %slice.66), channel_id=1, source_target_pairs={{0,16},{16,32},{32,48},{48,64},{64,80},{80,96},{96,112},{112,128},... | collective-permute-start | bytes 5768 | tf_op jit(solution)/shard_map/ppermute | solution.py:16
  13.7 4.3 %collective-permute-done = bf16[15,64]{0,1:T(8,128)(2,1)S(1)} collective-permute-done((bf16[15,64]{0,1:T(8,128)(2,1)S(1)}, bf16[15,64]{0,1:T(8,128)(2,1)S(1)}, u32[]{:S(2)}, u32[]{:S(2)}) %collective-permute-start) | collective-permute-done | bytes 1952 | tf_op jit(solution)/shard_map/ppermute | solution.py:16
  17.9 1.1 maximum_convert_fusion
  19.0 0.2 slice_add_fusion.2
  19.2 0.2 slice_add_fusion.1
  19.5 0.2 slice_add_fusion
  19.7 6.5 %convolution_convert_fusion = bf16[2048,2048]{1,0:T(8,128)(2,1)} fusion(bf16[64,2048]{1,0:T(8,128)(2,1)S(1)} %copy-done, f32[2063,64]{0,1:T(8,128)S(1)} %maximum_convert_fusion, f32[2062,64]{0,1:T(8,128)S(1)} %slice_add_fusion.2, f32[2060,64]{0,1:T(8,128)S(1)} %slice_add_fusion.1, f32[2056,64]{0,1:T(8,128)S(1)} %slice_add_fusion, f32[64]{0:T(128)S(1)} %copy-done.4, ...), kind=kOutput, calls=%fused_computation | convolution fusion | flops 542507008 | bytes 11283456 | tf_op jit(solution)/shard_map/dot_general | solution.py:108
  26.2 0.7 copy-done.3
  26.9 0.1 copy.29
  27.0 0.1 eq.138
  27.1 0.1 eq.134
  27.3 1.2 reduce-window.6
  28.5 0.2 slice_reduce_fusion
  28.8 0.1 reduce_sum.21
  29.0 0.3 fusion.6
  29.4 1.1 convolution_convert_fusion.1
  30.5 41.2 %all_to_all.19 = bf16[16,48,2048]{2,1,0:T(8,128)(2,1)S(1)} all-to-all(bf16[16,48,2048]{2,1,0:T(8,128)(2,1)S(1)} %bitcast.72), channel_id=1, replica_groups=mesh['ep'=16,'tp'=16] {'ep'}, dimensions={0} | all-to-all | bytes 6291456 | tf_op jit(solution)/shard_map/all_to_all | solution.py:123
  71.7 17.0 %all-gather.2.cloned.1.call-done = bf16[1024,6144]{1,0:T(8,128)(2,1)} async-done(((bf16[64,6144]{1,0:T(8,128)(2,1)}), bf16[1024,6144]{1,0:T(8,128)(2,1)}) %all-gather.2.cloned.1.call-update) | async-done | bytes 12582928 | tf_op jit(solution)/shard_map/all_gather | solution.py:22
  88.7 5.4 %fusion.1 = f32[768,1024]{1,0:T(8,128)S(1)} fusion(bf16[768,2048]{1,0:T(8,128)(2,1)S(1)} %bitcast.73, bf16[1024,6144]{1,0:T(8,128)(2,1)} %all-gather.2.cloned.1.call-done), kind=kOutput, calls=%fused_computation.4 | convolution fusion | flops 3221225472 | bytes 10485760 | tf_op jit(solution)/shard_map/erd,edf->erf/dot_general | solution.py:128
  94.1 0.4 copy-done.6
  94.6 3.9 %multiply_convert_fusion = bf16[768,1024]{1,0:T(8,128)(2,1)S(1)} fusion(f32[768,1024]{1,0:T(8,128)S(1)} %fusion.1, bf16[768,2048]{1,0:T(8,128)(2,1)S(1)} %bitcast.74, bf16[1024,6144]{1,0:T(8,128)(2,1)S(1)} %copy-done.6), kind=kOutput, calls=%fused_computation.10 | convolution fusion | flops 3225944064 | bytes 12058624 | tf_op jit(solution)/shard_map/erd,edf->erf/dot_general | solution.py:127
  98.4 3.6 %fusion.3 = bf16[768,2048]{1,0:T(8,128)(2,1)S(1)} fusion(bf16[768,1024]{1,0:T(8,128)(2,1)S(1)} %multiply_convert_fusion, bf16[1024,6144]{1,0:T(8,128)(2,1)S(1)} %copy-done.6), kind=kOutput, calls=%fused_computation.7 | convolution fusion | flops 3222798336 | bytes 8912896 | tf_op jit(solution)/shard_map/erf,edf->erd/dot_general | solution.py:130
  102.1 1.4 fusion.38
  103.5 28.0 %all_to_all.20 = bf16[16,1,24,2048]{3,2,1,0:T(8,128)(2,1)S(1)} all-to-all(bf16[16,1,24,2048]{3,2,1,0:T(8,128)(2,1)S(1)} %get-tuple-element.2), channel_id=1, replica_groups=mesh['ep'=16,'tp'=16] {'ep'}, dimensions={0} | all-to-all | bytes 3145728 | tf_op jit(solution)/shard_map/all_to_all | solution.py:52
  131.5 6.0 %all-to-all-start.2 = ((bf16[16,1,24,2048]{3,2,1,0:T(8,128)(2,1)}), bf16[16,1,24,2048]{3,2,1,0:T(8,128)(2,1)S(1)}, u32[]{:S(2)}, u32[]{:S(2)}) async-start(bf16[16,1,24,2048]{3,2,1,0:T(8,128)(2,1)} %get-tuple-element.3), calls=%async_computation.3 | async-start | bytes 3145728 | tf_op jit(solution)/shard_map/all_to_all | solution.py:52
  137.5 21.1 %all-to-all-done.2 = bf16[16,1,24,2048]{3,2,1,0:T(8,128)(2,1)S(1)} async-done(((bf16[16,1,24,2048]{3,2,1,0:T(8,128)(2,1)}), bf16[16,1,24,2048]{3,2,1,0:T(8,128)(2,1)S(1)}, u32[]{:S(2)}, u32[]{:S(2)}) %all-to-all-start.2) | async-done | bytes 1572896 | tf_op jit(solution)/shard_map/all_to_all | solution.py:52
  158.5 0.4 pad_maximum_fusion
  158.9 1.1 convolution_multiply_fusion.1
  160.0 2.1 %fusion.5 = bf16[256,2048]{1,0:T(8,128)(2,1)} fusion(f32[256,2048]{1,0:T(8,128)S(1)} %convolution_multiply_fusion.1, bf16[768,2048]{1,0:T(8,128)(2,1)S(1)} %bitcast.71, f32[256]{0:T(256)S(1)} %bitcast.81, s32[256]{0:T(256)S(1)} %bitcast.80), kind=kOutput, calls=%fused_computation.16 | convolution fusion | flops 807075840 | bytes 6293504 | tf_op jit(solution)/shard_map/dot_general | solution.py:137
  162.1 0.4 reduce-scatter.2.cloned.1.call-done
  (29 shorter events, 0.4 us)
Async XLA Ops:
  7.2 12.5 %copy-start = (bf16[64,2048]{1,0:T(8,128)(2,1)S(1)}, bf16[64,2048]{1,0:T(8,128)(2,1)}, u32[]{:S(2)}) copy-start(bf16[64,2048]{1,0:T(8,128)(2,1)} %param.12) | copy-start | bytes 786436
  7.2 81.5 %all-gather.2.cloned.1.call-start = ((), (), s32[]{:S(2)}) async-start(), calls=%async_computation.5 | async-start | bytes 13369344 | tf_op jit(solution)/shard_map/all_gather | solution.py:22
  9.3 10.4 %copy-start.4 = (f32[64]{0:T(128)S(1)}, f32[64]{0:T(128)}, u32[]{:S(2)}) copy-start(f32[64]{0:T(128)} %param.11) | copy-start | bytes 772
  9.3 153.2 %reduce-scatter.2.cloned.1.call-start = ((), (), s32[]{:S(2)}) async-start(), calls=%async_computation.4 | async-start | bytes 8912896 | tf_op jit(solution)/shard_map/reduce_scatter | solution.py:107
  10.2 7.7 %collective-permute-start = (bf16[15,64]{0,1:T(8,128)(2,1)S(1)}, bf16[15,64]{0,1:T(8,128)(2,1)S(1)}, u32[]{:S(2)}, u32[]{:S(2)}) collective-permute-start(bf16[15,64]{0,1:T(8,128)(2,1)S(1)} %slice.66), channel_id=1, source_target_pairs={{0,16},{16,32},{32,48},{48,64},{64,80},{80,96},{96,112},{112,128},... | collective-permute-start | bytes 5768 | tf_op jit(solution)/shard_map/ppermute | solution.py:16
  26.2 0.7 copy-start.3
  26.2 2.9 %copy-start.1 = (bf16[256,2048]{1,0:T(8,128)(2,1)S(1)}, bf16[256,2048]{1,0:T(8,128)(2,1)}, u32[]{:S(2)}) copy-start(bf16[256,2048]{1,0:T(8,128)(2,1)} %param.13) | copy-start | bytes 3145732
  26.2 3.2 %copy-start.2 = (f32[2048]{0:T(1024)S(1)}, f32[2048]{0:T(1024)}, u32[]{:S(2)}) copy-start(f32[2048]{0:T(1024)} %param.14) | copy-start | bytes 24580
  88.7 5.8 %copy-start.6 = (bf16[1024,6144]{1,0:T(8,128)(2,1)S(1)}, bf16[1024,6144]{1,0:T(8,128)(2,1)}, u32[]{:S(2)}) copy-start(bf16[1024,6144]{1,0:T(8,128)(2,1)} %all-gather.2.cloned.1.call-done) | copy-start | bytes 37748740
  103.5 34.0 %copy-start.5 = (f32[256,2]{0,1:T(2,128)S(1)}, f32[256,2]{0,1:T(2,128)}, u32[]{:S(2)}) copy-start(f32[256,2]{0,1:T(2,128)} %param.16) | copy-start | bytes 6148
  131.5 27.0 %all-to-all-start.2 = ((bf16[16,1,24,2048]{3,2,1,0:T(8,128)(2,1)}), bf16[16,1,24,2048]{3,2,1,0:T(8,128)(2,1)S(1)}, u32[]{:S(2)}, u32[]{:S(2)}) async-start(bf16[16,1,24,2048]{3,2,1,0:T(8,128)(2,1)} %get-tuple-element.3), calls=%async_computation.3 | async-start | bytes 3145728 | tf_op jit(solution)/shard_map/all_to_all | solution.py:52
Sparse Core Ops, SparseCore 0:
  10.4 78.2 all-gather.1
  91.8 70.6 reduce-scatter.1
where the time goes:
time: 170 us; the launch traced here: 169 us
  blocking collectives  69.2 us (41%)
  waiting for transfers between devices  42.8 us (25%)
  matrix products  23.8 us (14%)
  between operations  14.3 us (8%)
  starting transfers between devices  9.42 us (6%)
  other arithmetic  5.79 us (3%)
  local copies, waits for them, and re-layouts  4.17 us (2%)
    all_to_all x1, blocking collectives, body(): lax.all_to_all(outgoing, 'ep', split_axis=0, concat_axis=1, tiled=True)  41.2 us
    all_to_all x1, blocking collectives, exchange_in_pieces(): lax.all_to_all(section, axis, split_axis=0, concat_axis=0, tiled=True)  28 us
    all_to_all x1, waiting for transfers between devices, exchange_in_pieces(): lax.all_to_all(section, axis, split_axis=0, concat_axis=0, tiled=True)  21.1 us
    all_gather x1, waiting for transfers between devices, gather_turned(): lax.all_gather(both, axis, axis=0, tiled=True)  17 us
    dot_general x1, matrix products, body(): jnp.dot(pooled, mix_weight, preferred_element_type=jnp.float32)  6.48 us
    all_to_all x1, starting transfers between devices, exchange_in_pieces(): lax.all_to_all(section, axis, split_axis=0, concat_axis=0, tiled=True)  5.95 us
    dot_general x1, matrix products, body(): jnp.einsum('erd,edf->erf', arrived, up_piece, preferred_element_type=jnp....  5.42 us
    ppermute x1, waiting for transfers between devices, from_behind(): return lax.ppermute(shard, axis, pairs)  4.26 us
  transfers between devices with their start and end apart: 4, of which 4 were waited for; matrix products, arithmetic and copies ran while one was open for 18% of the time, Pallas kernels for 0%

commit v1 on v0

--- a/solution.py
+++ b/solution.py
@@ -19,7 +19,13 @@
 def gather_turned(arrays, axis, dims):
     turned = [jnp.moveaxis(a, dim, 0) for a, dim in zip(arrays, dims)]
     both = jnp.concatenate([t.reshape(len(t), -1) for t in turned], axis=1)
-    result, at, gathered = (lax.all_gather(both, axis, axis=0, tiled=True), 0, [])
+    result, at, gathered = (
+        jnp.concatenate(
+            lax.all_to_all(jnp.stack([both] * lax.axis_size(axis)), axis, 0, 0), axis=0
+        ),
+        0,
+        [],
+    )
     for t, dim in zip(turned, dims):
         section = result[:, at : at + t[0].size].reshape(-1, *t.shape[1:])
         gathered.append(jnp.moveaxis(section, 0, dim))

time: 170 us -> 486 us (2.86)
  waiting for transfers between devices: 42.8 us -> 373 us
  blocking collectives: 69.2 us -> 27 us
  starting transfers between devices: 9.42 us -> 24.1 us
  matrix products: 23.8 us -> 32.7 us
  local copies, waits for them, and re-layouts: 4.17 us -> 9.12 us
    all_to_all x0 -> x2, waiting for transfers between devices: none -> 346 us  [the longest x1 299 us: gather_turned(): lax.all_to_all(jnp.stack([both] * lax.axis_size(axis)), axis, 0, 0)]
    all_to_all x1 -> x0, blocking collectives: 41.2 us -> none  [body(): lax.all_to_all(outgoing, 'ep', split_axis=0, concat_axis=1, tiled=True)]
    all_gather x1 -> x0, waiting for transfers between devices: 17 us -> none  [gather_turned(): lax.all_gather(both, axis, axis=0, tiled=True)]
    all_to_all x0 -> x2, starting transfers between devices: none -> 16.1 us  [the longest x1 8.76 us: gather_turned(): lax.all_to_all(jnp.stack([both] * lax.axis_size(axis)), axis, 0, 0)]
    another operation x1 -> x2, local copies, waits for them, and re-layouts: 0.01 us -> 6.04 us  [the longest x1 6.04 us: gather_turned(): jnp.stack([both] * lax.axis_size(axis))]
  transfers between devices with their start and end apart: 4 -> 5, of which waited for: 4 -> 4; matrix products, arithmetic and copies ran while one was open for 18% -> 6% of each run, Pallas kernels for 0% -> 0%
where the time goes in v1:
time: 486 us; the launch traced here: 485 us
  waiting for transfers between devices  373 us (77%)
  matrix products  32.7 us (7%)
  blocking collectives  27 us (6%)
  starting transfers between devices  24.1 us (5%)
  between operations  14.2 us (3%)
  local copies, waits for them, and re-layouts  9.12 us (2%)
    all_to_all x1, waiting for transfers between devices, gather_turned(): lax.all_to_all(jnp.stack([both] * lax.axis_size(axis)), axis, 0, 0)  299 us
    all_to_all x1, waiting for transfers between devices, body(): lax.all_to_all(outgoing, 'ep', split_axis=0, concat_axis=1, tiled=True)  46.3 us
    all_to_all x1, blocking collectives, exchange_in_pieces(): lax.all_to_all(section, axis, split_axis=0, concat_axis=0, tiled=True)  27 us
    all_to_all x1, waiting for transfers between devices, exchange_in_pieces(): lax.all_to_all(section, axis, split_axis=0, concat_axis=0, tiled=True)  21.8 us
  transfers between devices with their start and end apart: 5, of which 4 were waited for; matrix products, arithmetic and copies ran while one was open for 6% of the time, Pallas kernels for 0%

profile of v1, /device:TPU:24, one launch (start us, length us, event | category | flops | bytes accessed | tf_op | source)
XLA Modules:
  0.0 484.8 jit_solution(15221966588826953785)
XLA Ops:
  7.2 0.9 copy.29
  8.0 0.1 eq.138
  8.2 0.1 eq.134
  8.3 1.2 reduce-window.6
  9.5 0.2 slice_reduce_fusion
  9.8 0.1 fusion.35
  9.9 0.1 reduce_sum.21
  10.1 0.7 multiply_add_fusion
  10.8 1.5 fusion.6
  12.3 4.0 convolution_convert_fusion.1
  16.3 7.3 %all-to-all-start = ((bf16[16,48,2048]{2,1,0:T(8,128)(2,1)}), bf16[16,48,2048]{2,1,0:T(8,128)(2,1)}, u32[]{:S(2)}, u32[]{:S(2)}) async-start(bf16[16,48,2048]{2,1,0:T(8,128)(2,1)} %bitcast.4), calls=%async_computation.1 | async-start | bytes 6291456 | tf_op jit(solution)/shard_map/all_to_all | solution.py:129
  23.7 46.3 %all-to-all-done = bf16[16,48,2048]{2,1,0:T(8,128)(2,1)} async-done(((bf16[16,48,2048]{2,1,0:T(8,128)(2,1)}), bf16[16,48,2048]{2,1,0:T(8,128)(2,1)}, u32[]{:S(2)}, u32[]{:S(2)}) %all-to-all-start) | async-done | bytes 3145760 | tf_op jit(solution)/shard_map/all_to_all | solution.py:129
  70.0 6.0 %stack.2 = bf16[16,64,6144]{2,1,0:T(8,128)(2,1)} broadcast(bf16[64,6144]{1,0:T(8,128)(2,1)S(1)} %pad_maximum_fusion.1), dimensions={1,2} | broadcast | bytes 13369344 | tf_op jit(solution)/shard_map/stack | solution.py:24
  76.0 8.8 %all-to-all-start.1 = ((bf16[16,64,6144]{2,1,0:T(8,128)(2,1)}), bf16[16,64,6144]{2,1,0:T(8,128)(2,1)}, u32[]{:S(2)}, u32[]{:S(2)}) async-start(bf16[16,64,6144]{2,1,0:T(8,128)(2,1)} %stack.2), calls=%async_computation.2 | async-start | bytes 25165824 | tf_op jit(solution)/shard_map/all_to_all | solution.py:24
  84.9 2.1 collective-permute-start
  87.1 5.6 %collective-permute-done = bf16[15,64]{0,1:T(8,128)(2,1)S(1)} collective-permute-done((bf16[15,64]{0,1:T(8,128)(2,1)S(1)}, bf16[15,64]{0,1:T(8,128)(2,1)S(1)}, u32[]{:S(2)}, u32[]{:S(2)}) %collective-permute-start) | collective-permute-done | bytes 1952 | tf_op jit(solution)/shard_map/ppermute | solution.py:16
  92.7 0.1 maximum_convert_fusion
  92.8 0.2 slice_add_fusion.2
  93.0 0.2 slice_add_fusion.1
  93.2 0.2 slice_add_fusion
  93.5 6.4 %convolution_convert_fusion = bf16[2048,2048]{1,0:T(8,128)(2,1)} fusion(bf16[64,2048]{1,0:T(8,128)(2,1)S(1)} %copy-done, f32[2063,64]{0,1:T(8,128)S(1)} %maximum_convert_fusion, f32[2062,64]{0,1:T(8,128)S(1)} %slice_add_fusion.2, f32[2060,64]{0,1:T(8,128)S(1)} %slice_add_fusion.1, f32[2056,64]{0,1:T(8,128)S(1)} %slice_add_fusion, f32[64]{0:T(128)S(1)} %copy-done.5, ...), kind=kOutput, calls=%fused_computation | convolution fusion | flops 542507008 | bytes 11283456 | tf_op jit(solution)/shard_map/dot_general | solution.py:114
  99.8 299.4 %all-to-all-done.1 = bf16[16,64,6144]{2,1,0:T(8,128)(2,1)} async-done(((bf16[16,64,6144]{2,1,0:T(8,128)(2,1)}), bf16[16,64,6144]{2,1,0:T(8,128)(2,1)}, u32[]{:S(2)}, u32[]{:S(2)}) %all-to-all-start.1) | async-done | bytes 12582944 | tf_op jit(solution)/shard_map/all_to_all | solution.py:24
  399.2 6.3 %fusion.1 = f32[768,1024]{1,0:T(8,128)S(1)} fusion(bf16[768,2048]{1,0:T(8,128)(2,1)} %bitcast.5, bf16[1024,6144]{1,0:T(8,128)(2,1)} %bitcast.12), kind=kOutput, calls=%fused_computation.4 | convolution fusion | flops 3221225472 | bytes 10485760 | tf_op jit(solution)/shard_map/erd,edf->erf/dot_general | solution.py:134
  405.6 7.0 %multiply_convert_fusion = bf16[768,1024]{1,0:T(8,128)(2,1)S(1)} fusion(f32[768,1024]{1,0:T(8,128)S(1)} %fusion.1, bf16[768,2048]{1,0:T(8,128)(2,1)} %bitcast.5, bf16[1024,6144]{1,0:T(8,128)(2,1)} %bitcast.12), kind=kOutput, calls=%fused_computation.10 | convolution fusion | flops 3225944064 | bytes 12058624 | tf_op jit(solution)/shard_map/erd,edf->erf/dot_general | solution.py:133
  412.6 5.8 %fusion.3 = bf16[768,2048]{1,0:T(8,128)(2,1)S(1)} fusion(bf16[768,1024]{1,0:T(8,128)(2,1)S(1)} %multiply_convert_fusion, bf16[1024,6144]{1,0:T(8,128)(2,1)} %bitcast.12), kind=kOutput, calls=%fused_computation.7 | convolution fusion | flops 3222798336 | bytes 8912896 | tf_op jit(solution)/shard_map/erf,edf->erd/dot_general | solution.py:136
  418.4 1.4 fusion.38
  419.8 27.0 %all_to_all.24 = bf16[16,1,24,2048]{3,2,1,0:T(8,128)(2,1)S(1)} all-to-all(bf16[16,1,24,2048]{3,2,1,0:T(8,128)(2,1)S(1)} %get-tuple-element.2), channel_id=1, replica_groups=mesh['ep'=16,'tp'=16] {'ep'}, dimensions={0} | all-to-all | bytes 3145728 | tf_op jit(solution)/shard_map/all_to_all | solution.py:58
  446.8 6.0 %all-to-all-start.3 = ((bf16[16,1,24,2048]{3,2,1,0:T(8,128)(2,1)}), bf16[16,1,24,2048]{3,2,1,0:T(8,128)(2,1)S(1)}, u32[]{:S(2)}, u32[]{:S(2)}) async-start(bf16[16,1,24,2048]{3,2,1,0:T(8,128)(2,1)} %get-tuple-element.3), calls=%async_computation.4 | async-start | bytes 3145728 | tf_op jit(solution)/shard_map/all_to_all | solution.py:58
  452.7 21.8 %all-to-all-done.3 = bf16[16,1,24,2048]{3,2,1,0:T(8,128)(2,1)S(1)} async-done(((bf16[16,1,24,2048]{3,2,1,0:T(8,128)(2,1)}), bf16[16,1,24,2048]{3,2,1,0:T(8,128)(2,1)S(1)}, u32[]{:S(2)}, u32[]{:S(2)}) %all-to-all-start.3) | async-done | bytes 1572896 | tf_op jit(solution)/shard_map/all_to_all | solution.py:58
  474.6 0.2 pad_maximum_fusion
  474.8 1.1 convolution_multiply_fusion.1
  475.9 2.1 fusion.5
  (30 shorter events, 0.4 us)
Async XLA Ops:
  7.2 86.3 %copy-start = (bf16[64,2048]{1,0:T(8,128)(2,1)S(1)}, bf16[64,2048]{1,0:T(8,128)(2,1)}, u32[]{:S(2)}) copy-start(bf16[64,2048]{1,0:T(8,128)(2,1)} %param.12) | copy-start | bytes 786436
  16.3 7.3 %copy-start.2 = (bf16[1,2048,64]{1,2,0:T(8,128)(2,1)S(1)}, bf16[1,2048,64]{1,2,0:T(8,128)(2,1)}, u32[]{:S(2)}) copy-start(bf16[1,2048,64]{1,2,0:T(8,128)(2,1)} %param.19) | copy-start | bytes 786436
  16.3 7.3 %copy-start.3 = (bf16[1,2048,64]{1,2,0:T(8,128)(2,1)S(1)}, bf16[1,2048,64]{1,2,0:T(8,128)(2,1)}, u32[]{:S(2)}) copy-start(bf16[1,2048,64]{1,2,0:T(8,128)(2,1)} %param.18) | copy-start | bytes 786436
  16.3 7.3 %copy-start.4 = (bf16[1,2048,64]{1,2,0:T(8,128)(2,1)S(1)}, bf16[1,2048,64]{1,2,0:T(8,128)(2,1)}, u32[]{:S(2)}) copy-start(bf16[1,2048,64]{1,2,0:T(8,128)(2,1)} %param.17) | copy-start | bytes 786436
  16.3 53.6 %all-to-all-start = ((bf16[16,48,2048]{2,1,0:T(8,128)(2,1)}), bf16[16,48,2048]{2,1,0:T(8,128)(2,1)}, u32[]{:S(2)}, u32[]{:S(2)}) async-start(bf16[16,48,2048]{2,1,0:T(8,128)(2,1)} %bitcast.4), calls=%async_computation.1 | async-start | bytes 6291456 | tf_op jit(solution)/shard_map/all_to_all | solution.py:129
  76.0 8.8 %copy-start.1 = (bf16[2048,64]{0,1:T(8,128)(2,1)S(1)}, bf16[2048,64]{0,1:T(8,128)(2,1)}, u32[]{:S(2)}) copy-start(bf16[2048,64]{0,1:T(8,128)(2,1)} %param.10) | copy-start | bytes 786436
  76.0 323.2 %all-to-all-start.1 = ((bf16[16,64,6144]{2,1,0:T(8,128)(2,1)}), bf16[16,64,6144]{2,1,0:T(8,128)(2,1)}, u32[]{:S(2)}, u32[]{:S(2)}) async-start(bf16[16,64,6144]{2,1,0:T(8,128)(2,1)} %stack.2), calls=%async_computation.2 | async-start | bytes 25165824 | tf_op jit(solution)/shard_map/all_to_all | solution.py:24
  84.8 8.7 %copy-start.5 = (f32[64]{0:T(128)S(1)}, f32[64]{0:T(128)}, u32[]{:S(2)}) copy-start(f32[64]{0:T(128)} %param.11) | copy-start | bytes 772
  84.8 393.2 %reduce-scatter.2.cloned.1.call-start = ((), (), s32[]{:S(2)}) async-start(), calls=%async_computation.5 | async-start | bytes 8912896 | tf_op jit(solution)/shard_map/reduce_scatter | solution.py:113
  84.9 7.7 %collective-permute-start = (bf16[15,64]{0,1:T(8,128)(2,1)S(1)}, bf16[15,64]{0,1:T(8,128)(2,1)S(1)}, u32[]{:S(2)}, u32[]{:S(2)}) collective-permute-start(bf16[15,64]{0,1:T(8,128)(2,1)S(1)} %slice.66), channel_id=1, source_target_pairs={{0,16},{16,32},{32,48},{48,64},{64,80},{80,96},{96,112},{112,128},... | collective-permute-start | bytes 5768 | tf_op jit(solution)/shard_map/ppermute | solution.py:16
  419.8 32.9 %copy-start.6 = (f32[256,2]{0,1:T(2,128)S(1)}, f32[256,2]{0,1:T(2,128)}, u32[]{:S(2)}) copy-start(f32[256,2]{0,1:T(2,128)} %param.16) | copy-start | bytes 6148
  446.8 27.8 %all-to-all-start.3 = ((bf16[16,1,24,2048]{3,2,1,0:T(8,128)(2,1)}), bf16[16,1,24,2048]{3,2,1,0:T(8,128)(2,1)S(1)}, u32[]{:S(2)}, u32[]{:S(2)}) async-start(bf16[16,1,24,2048]{3,2,1,0:T(8,128)(2,1)} %get-tuple-element.3), calls=%async_computation.4 | async-start | bytes 3145728 | tf_op jit(solution)/shard_map/all_to_all | solution.py:58
Sparse Core Ops, SparseCore 0:
  100.0 301.9 reduce-scatter.1
